TPU v7x, 32 devices: a whole 2x2x4 slice. The times are simulated.
32 devices in a mesh: fs: 8 (over z, x), tp: 4 (over y, core).
Axes of the slice: x: 2, y: 2, z: 4, core: 2. Of those that a mesh axis runs over, the one named last changes fastest.
Arguments:
- later_in: bfloat16 [8192, 2048], P('fs'), may hold values from -3 to 3
- earlier_in: bfloat16 [8192, 2048], P('fs'), may hold values from -3 to 3
- cotangent: bfloat16 [8192, 2048], P('fs'), may hold values from -6 to 6
- gate_weight: bfloat16 [2048, 5632], P('fs', 'tp'), may hold values from -0.125 to 0.125
- up_weight: bfloat16 [2048, 5632], P('fs', 'tp'), may hold values from -0.125 to 0.125
- down_weight: bfloat16 [2048, 5632], P('fs', 'tp'), may hold values from -0.078125 to 0.078125
- norm_gain: bfloat16 [2048], replicated, may hold values from 0.099609375 to 1.8984375
- gate_sum: float32 [2048, 5632], P('fs', 'tp'), may hold values from -96 to 96
- up_sum: float32 [2048, 5632], P('fs', 'tp'), may hold values from -96 to 96
- down_sum: float32 [2048, 5632], P('fs', 'tp'), may hold values from -96 to 96
- gain_sum: float32 [2048], replicated, may hold values from -192 to 192
Outputs:
- later_out: bfloat16 [8192, 2048], P(('fs', 'tp'))
- later_hidden: bfloat16 [8192, 5632], P('fs', 'tp')
- earlier_grad: bfloat16 [8192, 2048], P(('fs', 'tp'))
- gate_sum_new: float32 [2048, 5632], P('fs', 'tp')
- up_sum_new: float32 [2048, 5632], P('fs', 'tp')
- down_sum_new: float32 [2048, 5632], P('fs', 'tp')
- gain_sum_new: float32 [2048], replicated
All inputs are finite; a program needn't handle non-finite values.
Results may differ from a plain program's by a relative error of at most 0.013.
Values may be sent and summed in bfloat16 or wider, within the bound.
No kernel may reach another device: no remote copies, remote signals or barrier semaphores. Data moves between devices by JAX's collectives and lax.ppermute only.
A program may use at most 128 MiB of HBM per device.

v0:
```python
import jax
import jax.numpy as jnp
from jax import lax
from jax.sharding import PartitionSpec as P

norm_floor = 0.05


def normalize(tokens_in, norm_gain):
    values = tokens_in.astype(jnp.float32)
    row_scale = lax.rsqrt(jnp.mean(values * values, axis=1, keepdims=True) + norm_floor)
    unit_rows = values * row_scale
    normed = (unit_rows * norm_gain.astype(jnp.float32)).astype(jnp.bfloat16)
    return (row_scale, unit_rows, normed)


def transposed(matrix_a, matrix_b):
    return lax.dot_general(
        matrix_a, matrix_b, (((1,), (1,)), ((), ())), preferred_element_type=jnp.float32
    )


def outer_sum(matrix_a, matrix_b):
    return lax.dot_general(
        matrix_a, matrix_b, (((0,), (0,)), ((), ())), preferred_element_type=jnp.float32
    )


def own_rows(tokens_in, own_count):
    return lax.dynamic_slice_in_dim(tokens_in, lax.axis_index("tp") * own_count, own_count, 0)


def forward(later_in, norm_gain, weights):
    w_gate, w_up, w_down = weights
    normed = normalize(later_in, norm_gain)[2]
    gate_pre = jnp.dot(normed, w_gate, preferred_element_type=jnp.float32)
    up_pre = jnp.dot(normed, w_up, preferred_element_type=jnp.float32)
    hidden = (jax.nn.silu(gate_pre) * up_pre).astype(jnp.bfloat16)
    own_count = later_in.shape[0] // lax.axis_size("tp")
    summed = lax.psum_scatter(
        transposed(hidden, w_down).astype(jnp.bfloat16), "tp", scatter_dimension=0, tiled=True
    ).astype(jnp.float32)
    later_out = (own_rows(later_in, own_count).astype(jnp.float32) + 0.5 * summed).astype(
        jnp.bfloat16
    )
    return (later_out, hidden)


def backward(earlier_in, cotangent, norm_gain, weights):
    w_gate, w_up, w_down = weights
    row_scale, unit_rows, normed = normalize(earlier_in, norm_gain)
    gate_pre = jnp.dot(normed, w_gate, preferred_element_type=jnp.float32)
    up_pre = jnp.dot(normed, w_up, preferred_element_type=jnp.float32)
    sigmoid_gate = jax.nn.sigmoid(gate_pre)
    activated = gate_pre * sigmoid_gate
    hidden = (activated * up_pre).astype(jnp.bfloat16)
    col_width = hidden.shape[1]
    dhidden = jnp.dot(cotangent, w_down, preferred_element_type=jnp.float32)
    dgate = (
        0.5 * dhidden * up_pre * sigmoid_gate * (1.0 + gate_pre * (1.0 - sigmoid_gate))
    ).astype(jnp.bfloat16)
    dupper = (0.5 * dhidden * activated).astype(jnp.bfloat16)
    gate_and_up = jnp.concatenate([dgate, dupper], axis=1)
    dnormed = transposed(dgate, w_gate) + transposed(dupper, w_up)
    gain_part = jnp.sum(dnormed * unit_rows, axis=0)
    weighted = dnormed * norm_gain.astype(jnp.float32)
    branch = row_scale * (
        weighted - unit_rows * jnp.mean(weighted * unit_rows, axis=1, keepdims=True)
    )
    own_count = earlier_in.shape[0] // lax.axis_size("tp")
    summed = lax.psum_scatter(
        branch.astype(jnp.bfloat16), "tp", scatter_dimension=0, tiled=True
    ).astype(jnp.float32)
    earlier_grad = (own_rows(cotangent, own_count).astype(jnp.float32) + summed).astype(
        jnp.bfloat16
    )
    grads_total = lax.psum_scatter(
        jnp.concatenate(
            [outer_sum(normed, gate_and_up), 0.5 * outer_sum(cotangent, hidden)], axis=1
        ).astype(jnp.bfloat16),
        "fs",
        scatter_dimension=0,
        tiled=True,
    ).astype(jnp.float32)
    grad_gate = grads_total[:, :col_width]
    grad_up = grads_total[:, col_width : 2 * col_width]
    grad_down = grads_total[:, 2 * col_width :]
    gain_total = lax.psum(gain_part, ("fs", "tp"))
    return (earlier_grad, grad_gate, grad_up, grad_down, gain_total)


def local(
    later_in,
    earlier_in,
    cotangent,
    gate_weight,
    up_weight,
    down_weight,
    norm_gain,
    gate_sum,
    up_sum,
    down_sum,
    gain_sum,
):
    pieces = (gate_weight, up_weight, down_weight)
    later_out, later_hidden = forward(
        later_in,
        norm_gain,
        (
            lax.all_gather(pieces[0], "fs", axis=0, tiled=True),
            lax.all_gather(pieces[1], "fs", axis=0, tiled=True),
            lax.all_gather(pieces[2], "fs", axis=0, tiled=True),
        ),
    )
    earlier = backward(
        earlier_in,
        cotangent,
        norm_gain,
        (
            lax.all_gather(pieces[0], "fs", axis=0, tiled=True),
            lax.all_gather(pieces[1], "fs", axis=0, tiled=True),
            lax.all_gather(pieces[2], "fs", axis=0, tiled=True),
        ),
    )
    earlier_grad, grad_gate, grad_up, grad_down, gain_total = earlier
    return (
        later_out,
        later_hidden,
        earlier_grad,
        gate_sum + grad_gate,
        up_sum + grad_up,
        down_sum + grad_down,
        gain_sum + gain_total,
    )


def solution(mesh):
    placed = (
        P("fs", None),
        P("fs", None),
        P("fs", None),
        P("fs", "tp"),
        P("fs", "tp"),
        P("fs", "tp"),
        P(),
        P("fs", "tp"),
        P("fs", "tp"),
        P("fs", "tp"),
        P(),
    )
    return jax.shard_map(
        local,
        mesh=mesh,
        in_specs=placed,
        out_specs=(
            P(("fs", "tp"), None),
            P("fs", "tp"),
            P(("fs", "tp"), None),
            P("fs", "tp"),
            P("fs", "tp"),
            P("fs", "tp"),
            P(),
        ),
        check_vma=False,
    )
```

profile of v0, /device:TPU:0, one launch (start us, length us, event | category | flops | bytes accessed | tf_op | source)
XLA Modules:
  0.0 708.4 jit_solution(3213249192349217438)
XLA Ops:
  7.2 0.0 all-gather.4.cloned.1.call-start
  7.2 0.7 all-gather.4.cloned.1.call-update
  7.9 0.0 all-gather.6.cloned.1.call-start
  7.9 0.7 all-gather.6.cloned.1.call-update
  8.7 0.0 all-gather.8.cloned.1.call-start
  8.7 0.7 all-gather.8.cloned.1.call-update
  9.4 0.0 reduce-scatter.4.cloned.1.call-start
  9.4 0.0 copy-start
  9.4 0.8 convert_element_type.59
  10.3 3.3 fusion.4
  13.6 0.0 copy-done
  13.6 0.9 fusion.13
  14.5 90.8 %all-gather.4.cloned.1.call-done = bf16[2048,1408]{1,0:T(8,128)(2,1)} async-done(((bf16[256,1408]{1,0:T(8,128)(2,1)}), bf16[2048,1408]{1,0:T(8,128)(2,1)}) %all-gather.4.cloned.1.call-update) | async-done | bytes 5767184 | tf_op jit(solution)/shard_map/all_gather | solution.py:110
  105.2 12.0 %fusion.20 = f32[1024,1408]{1,0:T(8,128)} fusion(bf16[2048,1408]{1,0:T(8,128)(2,1)} %all-gather.4.cloned.1.call-done, bf16[1024,2048]{1,0:T(8,128)(2,1)} %param.11, f32[2048]{0:T(1024)S(1)} %convert_element_type.59, f32[1024]{0:T(1024)S(1)} %add_rsqrt_fusion.1), kind=kOutput, calls=%fused_computation.38 | convolution fusion | flops 5913968640 | bytes 15740928 | tf_op jit(solution)/shard_map/dot_general | solution.py:36
  117.2 80.8 %all-gather.6.cloned.1.call-done = bf16[2048,1408]{1,0:T(8,128)(2,1)} async-done(((bf16[256,1408]{1,0:T(8,128)(2,1)}), bf16[2048,1408]{1,0:T(8,128)(2,1)}) %all-gather.6.cloned.1.call-update) | async-done | bytes 5767184 | tf_op jit(solution)/shard_map/all_gather | solution.py:111
  197.9 11.3 %multiply_convert_fusion.4 = bf16[1024,1408]{1,0:T(8,128)(2,1)S(1)} fusion(f32[1024,1408]{1,0:T(8,128)} %fusion.20, bf16[2048,1408]{1,0:T(8,128)(2,1)} %all-gather.6.cloned.1.call-done, bf16[1024,2048]{1,0:T(8,128)(2,1)} %param.11, f32[2048]{0:T(1024)S(1)} %convert_element_type.59, f32[1024]{0:T(1024)S(1)} %add_rsqrt_fusion.1), kind=kOutput, calls=%fused_computation.30 | convolution fusion | flops 5922619392 | bytes 18624512 | tf_op jit(solution)/shard_map/dot_general | solution.py:37
  209.2 0.0 copy-start.8
  209.3 81.4 %all-gather.8.cloned.1.call-done = bf16[2048,1408]{1,0:T(8,128)(2,1)} async-done(((bf16[256,1408]{1,0:T(8,128)(2,1)}), bf16[2048,1408]{1,0:T(8,128)(2,1)}) %all-gather.8.cloned.1.call-update) | async-done | bytes 5767184 | tf_op jit(solution)/shard_map/all_gather | solution.py:112
  290.6 10.9 %convolution_convert_fusion.1 = bf16[1024,2048]{1,0:T(8,128)(2,1)} fusion(bf16[1024,1408]{1,0:T(8,128)(2,1)S(1)} %multiply_convert_fusion.4, bf16[2048,1408]{1,0:T(8,128)(2,1)} %all-gather.8.cloned.1.call-done), kind=kOutput, calls=%fused_computation.32 | convolution fusion | flops 5907677184 | bytes 12845056 | tf_op jit(solution)/shard_map/dot_general | solution.py:18
  301.5 0.0 copy-done.8
  301.5 0.0 reduce-scatter.4.cloned.1.call-update
  301.5 0.2 reduce-scatter.6.cloned.1.call-start
  301.8 0.0 copy-start.1
  301.8 0.0 slice-start.2
  301.8 12.1 %fusion.26 = f32[1024,1408]{1,0:T(8,128)} fusion(bf16[2048,1408]{1,0:T(8,128)(2,1)} %all-gather.4.cloned.1.call-done, bf16[1024,2048]{1,0:T(8,128)(2,1)} %param.12, f32[1024]{0:T(1024)S(1)} %add_rsqrt_fusion, f32[2048]{0:T(1024)S(1)} %convert_element_type.59), kind=kOutput, calls=%fused_computation.44 | convolution fusion | flops 5913968640 | bytes 15740928 | tf_op jit(solution)/shard_map/dot_general | solution.py:52
  313.9 0.0 copy-done.1
  313.9 0.0 copy-start.6
  313.9 0.0 slice-start.3
  313.9 0.0 slice-start
  313.9 10.7 %fusion.28 = f32[1024,1408]{1,0:T(8,128)} fusion(bf16[2048,1408]{1,0:T(8,128)(2,1)} %all-gather.6.cloned.1.call-done, bf16[1024,2048]{1,0:T(8,128)(2,1)S(1)} %copy-done.1, f32[1024]{0:T(1024)S(1)} %add_rsqrt_fusion, f32[2048]{0:T(1024)S(1)} %convert_element_type.59), kind=kOutput, calls=%fused_computation.45 | convolution fusion | flops 5913968640 | bytes 15740928 | tf_op jit(solution)/shard_map/dot_general | solution.py:53
  324.6 0.0 slice-done.2
  324.6 0.0 copy-done.6
  324.6 0.0 slice-done.3
  324.7 0.0 slice-start.1
  324.7 12.3 %multiply_convert_fusion.2 = (bf16[1024,1408]{1,0:T(8,128)(2,1)S(1)}, bf16[1024,1408]{1,0:T(8,128)(2,1)}) fusion(f32[1024,1408]{1,0:T(8,128)} %fusion.26, f32[1024,1408]{1,0:T(8,128)} %fusion.28, bf16[1024,2048]{1,0:T(8,128)(2,1)S(1)} %copy-done.6, bf16[2048,1408]{1,0:T(8,128)(2,1)S(1)} %bitcast.18), kind=kOutput, calls=%fused_computation.26 | convolution fusion | flops 5925765120 | bytes 27262976 | tf_op jit(solution)/shard_map/dot_general | solution.py:58
  337.0 0.0 slice-done
  337.0 0.0 slice-done.1
  337.0 10.2 %fusion.30 = f32[1024,2048]{1,0:T(8,128)} fusion(bf16[1024,1408]{1,0:T(8,128)(2,1)} %get-tuple-element.10, bf16[2048,1408]{1,0:T(8,128)(2,1)S(1)} %bitcast.16), kind=kOutput, calls=%fused_computation.46 | convolution fusion | flops 5905580032 | bytes 17039360 | tf_op jit(solution)/shard_map/dot_general | solution.py:18
  347.2 11.1 %fusion.12 = (f32[2048]{0:T(1024)S(1)}, f32[1024]{0:T(1024)S(1)}, f32[1024,2048]{1,0:T(8,128)S(1)}) fusion(bf16[1024,2048]{1,0:T(8,128)(2,1)S(1)} %copy-done.1, f32[1024]{0:T(1024)S(1)} %add_rsqrt_fusion, f32[2048]{0:T(1024)S(1)} %convert_element_type.59, f32[1024,2048]{1,0:T(8,128)} %fusion.30, bf16[1024,1408]{1,0:T(8,128)(2,1)S(1)} %get-tuple-element.9, ...), kind=kOutput, calls=%fused_computation.19 | convolution fusion | flops 5922354176 | bytes 29646848 | tf_op jit(solution)/shard_map/dot_general | solution.py:18
  358.3 3.5 fusion.11
  361.8 0.0 reduce-scatter.6.cloned.1.call-update
  361.9 0.0 reduce-scatter.8.cloned.1.call-start
  361.9 0.0 copy-start.2
  361.9 13.0 %fusion.14 = bf16[2048,1408]{1,0:T(8,128)(2,1)S(1)} fusion(bf16[1024,2048]{1,0:T(8,128)(2,1)} %param.13, f32[1024,1408]{1,0:T(8,128)} %fusion.28, f32[1024,1408]{1,0:T(8,128)} %fusion.26), kind=kOutput, calls=%fused_computation.21 | convolution fusion | flops 5919997952 | bytes 21495808 | tf_op jit(solution)/shard_map/dot_general | solution.py:24
  374.9 0.0 copy-done.2
  374.9 17.4 %convolution_convert_fusion = bf16[2048,2816]{1,0:T(8,128)(2,1)} fusion(bf16[1024,1408]{1,0:T(8,128)(2,1)S(1)} %get-tuple-element.9, bf16[1024,1408]{1,0:T(8,128)(2,1)} %get-tuple-element.10, bf16[1024,2048]{1,0:T(8,128)(2,1)S(1)} %copy-done.2, f32[1024]{0:T(1024)S(1)} %add_rsqrt_fusion, f32[2048]{0:T(1024)S(1)} %convert_element_type.59), kind=kOutput, calls=%fused_computation.2 | convolution fusion | flops 11836850176 | bytes 21508096 | tf_op jit(solution)/shard_map/dot_general | solution.py:24
  392.3 11.8 %pad_maximum_fusion = bf16[2048,4224]{1,0:T(8,128)(2,1)} fusion(bf16[2048,1408]{1,0:T(8,128)(2,1)S(1)} %fusion.14, bf16[2048,2816]{1,0:T(8,128)(2,1)} %convolution_convert_fusion), kind=kLoop, calls=%fused_computation | loop fusion | flops 34603008 | bytes 34603008 | tf_op jit(solution)/shard_map/concatenate | solution.py:78
  404.1 0.0 copy-start.7
  404.1 0.0 reduce-scatter.8.cloned.1.call-update
  404.1 41.4 %psum.7 = f32[2048]{0:T(1024)S(1)} all-reduce(f32[2048]{0:T(1024)S(1)} %get-tuple-element.7), channel_id=1, replica_groups=mesh['fs'=8,'tp'=4] {'fs','tp'}, use_global_device_ids=true, to_apply=%region_7.8 | all-reduce | flops 2048 | bytes 16384 | tf_op jit(solution)/shard_map/psum | solution.py:88
  445.5 0.0 copy-done.7
  445.5 0.6 add.71
  446.1 0.0 copy-start.3
  446.1 0.0 copy-start.4
  446.1 0.0 reduce-scatter.4.cloned.1.call-done
  446.1 3.1 add_convert_fusion.1
  449.2 0.0 reduce-scatter.6.cloned.1.call-done
  449.2 2.9 add_convert_fusion
  452.2 245.1 %reduce-scatter.8.cloned.1.call-done = bf16[256,4224]{1,0:T(8,128)(2,1)} async-done(((bf16[2048,4224]{1,0:T(8,128)(2,1)}), bf16[256,4224]{1,0:T(8,128)(2,1)}) %reduce-scatter.8.cloned.1.call-update) | async-done | bytes 2162704 | tf_op jit(solution)/shard_map/reduce_scatter | solution.py:77
  697.2 2.0 convert_element_type.74
  699.2 0.0 copy-done.3
  699.2 0.0 copy-done.4
  699.3 0.0 copy-done.5
  699.3 2.3 slice_add_fusion
  (6 shorter events, 0.0 us)
Async XLA Ops:
  7.2 98.1 %all-gather.4.cloned.1.call-start = ((), (), s32[]{:S(2)}) async-start(), calls=%async_computation.3 | async-start | bytes 6488064 | tf_op jit(solution)/shard_map/all_gather | solution.py:110
  7.9 190.0 %all-gather.6.cloned.1.call-start = ((), (), s32[]{:S(2)}) async-start(), calls=%async_computation.4 | async-start | bytes 6488064 | tf_op jit(solution)/shard_map/all_gather | solution.py:111
  8.7 282.0 %all-gather.8.cloned.1.call-start = ((), (), s32[]{:S(2)}) async-start(), calls=%async_computation.5 | async-start | bytes 6488064 | tf_op jit(solution)/shard_map/all_gather | solution.py:112
  9.4 436.8 %reduce-scatter.4.cloned.1.call-start = ((), (), s32[]{:S(2)}) async-start(), calls=%async_computation.6 | async-start | bytes 5242880 | tf_op jit(solution)/shard_map/reduce_scatter | solution.py:40
  9.4 4.1 copy-start
  209.2 92.3 %copy-start.8 = (bf16[1024,1408]{1,0:T(8,128)(2,1)}, bf16[1024,1408]{1,0:T(8,128)(2,1)S(1)}, u32[]{:S(2)}) copy-start(bf16[1024,1408]{1,0:T(8,128)(2,1)S(1)} %multiply_convert_fusion.4) | copy-start | bytes 8650756
  301.5 147.7 %reduce-scatter.6.cloned.1.call-start = ((), (), s32[]{:S(2)}) async-start(), calls=%async_computation.7 | async-start | bytes 5242880 | tf_op jit(solution)/shard_map/reduce_scatter | solution.py:71
  301.8 12.2 %copy-start.1 = (bf16[1024,2048]{1,0:T(8,128)(2,1)S(1)}, bf16[1024,2048]{1,0:T(8,128)(2,1)}, u32[]{:S(2)}) copy-start(bf16[1024,2048]{1,0:T(8,128)(2,1)} %param.12) | copy-start | bytes 12582916
  301.8 22.9 %slice-start.2 = ((s8[5767168]{0:T(1024)(128)(4,1)}), s8[4194304]{0:T(1024)(128)(4,1)S(1)}, s32[]{:S(2)}) async-start(s8[5767168]{0:T(1024)(128)(4,1)} %bitcast.17), calls=%async_computation.11 | async-start | bytes 8388608
  313.9 10.7 %copy-start.6 = (bf16[1024,2048]{1,0:T(8,128)(2,1)S(1)}, bf16[1024,2048]{1,0:T(8,128)(2,1)}, u32[]{:S(2)}) copy-start(bf16[1024,2048]{1,0:T(8,128)(2,1)} %param.13) | copy-start | bytes 12582916
  313.9 10.7 %slice-start.3 = ((s8[5767168]{0:T(1024)(128)(4,1)}), s8[1572864]{0:T(1024)(128)(4,1)S(1)}, s32[]{:S(2)}) async-start(s8[5767168]{0:T(1024)(128)(4,1)} %bitcast.17), calls=%async_computation.12 | async-start | bytes 3145728
  313.9 23.0 %slice-start = ((s8[5767168]{0:T(1024)(128)(4,1)}), s8[4194304]{0:T(1024)(128)(4,1)S(1)}, s32[]{:S(2)}) async-start(s8[5767168]{0:T(1024)(128)(4,1)} %bitcast.15), calls=%async_computation.9 | async-start | bytes 8388608
  324.7 12.3 %slice-start.1 = ((s8[5767168]{0:T(1024)(128)(4,1)}), s8[1572864]{0:T(1024)(128)(4,1)S(1)}, s32[]{:S(2)}) async-start(s8[5767168]{0:T(1024)(128)(4,1)} %bitcast.15), calls=%async_computation.10 | async-start | bytes 3145728
  361.9 335.4 %reduce-scatter.8.cloned.1.call-start = ((), (), s32[]{:S(2)}) async-start(), calls=%async_computation.8 | async-start | bytes 19464192 | tf_op jit(solution)/shard_map/reduce_scatter | solution.py:77
  361.9 13.0 %copy-start.2 = (bf16[1024,2048]{1,0:T(8,128)(2,1)S(1)}, bf16[1024,2048]{1,0:T(8,128)(2,1)}, u32[]{:S(2)}) copy-start(bf16[1024,2048]{1,0:T(8,128)(2,1)} %param.12) | copy-start | bytes 12582916
  404.1 41.5 %copy-start.7 = (f32[2048]{0:T(1024)S(1)}, f32[2048]{0:T(1024)}, u32[]{:S(2)}) copy-start(f32[2048]{0:T(1024)} %param.21) | copy-start | bytes 24580
  446.1 253.1 %copy-start.3 = (f32[256,1408]{1,0:T(8,128)S(1)}, f32[256,1408]{1,0:T(8,128)}, u32[]{:S(2)}) copy-start(f32[256,1408]{1,0:T(8,128)} %param.20) | copy-start | bytes 4325380
  446.1 253.1 %copy-start.4 = (f32[256,1408]{1,0:T(8,128)S(1)}, f32[256,1408]{1,0:T(8,128)}, u32[]{:S(2)}) copy-start(f32[256,1408]{1,0:T(8,128)} %param.19) | copy-start | bytes 4325380
  697.2 2.0 copy-start.5
Sparse Core Ops, SparseCore 0:
  10.2 95.0 all-gather.3
  107.4 90.4 all-gather.5
  200.1 90.4 all-gather.7
  301.6 42.7 reduce-scatter.3
  362.0 42.7 reduce-scatter.5
  408.6 288.6 reduce-scatter.7
where the time goes:
time: 709 us; the launch traced here: 708 us
  waiting for transfers between devices  500 us (71%)
  matrix products  121 us (17%)
  blocking collectives  41.4 us (6%)
  other arithmetic  31.1 us (4%)
  between operations  14.3 us (2%)
    reduce_scatter x1, waiting for transfers between devices, backward(): lax.psum_scatter(jnp.concatenate([outer_sum(normed, gate_and_up), 0.5 * o...  245 us
    all_gather x1, waiting for transfers between devices, local(): lax.all_gather(pieces[0], 'fs', axis=0, tiled=True)  90.8 us
    all_gather x1, waiting for transfers between devices, local(): lax.all_gather(pieces[2], 'fs', axis=0, tiled=True)  81.4 us
    all_gather x1, waiting for transfers between devices, local(): lax.all_gather(pieces[1], 'fs', axis=0, tiled=True)  80.8 us
    psum x1, blocking collectives, backward(): gain_total = lax.psum(gain_part, ('fs', 'tp'))  41.4 us
    dot_general x3, matrix products, transposed(): lax.dot_general(matrix_a, matrix_b, (((1,), (1,)), ((), ())), preferred_e...  32.2 us
    dot_general x2, matrix products, outer_sum(): lax.dot_general(matrix_a, matrix_b, (((0,), (0,)), ((), ())), preferred_e...  30.4 us
  transfers between devices with their start and end apart: 6, of which 4 were waited for; matrix products, arithmetic and copies ran while one was open for 19% of the time, Pallas kernels for 0%

commit v1 on v0

--- a/solution.py
+++ b/solution.py
@@ -85,7 +85,7 @@
     grad_gate = grads_total[:, :col_width]
     grad_up = grads_total[:, col_width : 2 * col_width]
     grad_down = grads_total[:, 2 * col_width :]
-    gain_total = lax.psum(gain_part, ("fs", "tp"))
+    gain_total = lax.all_gather(gain_part, axis_name=("fs", "tp")).sum(axis=0)
     return (earlier_grad, grad_gate, grad_up, grad_down, gain_total)
 
 

time: 709 us -> 708 us (level)
    psum x1 -> x0, blocking collectives: 41.4 us -> none  [backward(): gain_total = lax.psum(gain_part, ('fs', 'tp'))]
    all_gather x0 -> x1, blocking collectives: none -> 40.9 us  [backward(): gain_total = lax.all_gather(gain_part, axis_name=('fs', 'tp')).sum(axis=0)]
where the time goes in v1:
time: 708 us
  waiting for transfers between devices  500 us (71%)
  matrix products  120 us (17%)
  blocking collectives  40.9 us (6%)
  other arithmetic  31.1 us (4%)
  between operations  14.3 us (2%)
    reduce_scatter x1, waiting for transfers between devices, backward(): lax.psum_scatter(jnp.concatenate([outer_sum(normed, gate_and_up), 0.5 * o...  245 us
    all_gather x1, waiting for transfers between devices, local(): lax.all_gather(pieces[0], 'fs', axis=0, tiled=True)  90.8 us
    all_gather x1, waiting for transfers between devices, local(): lax.all_gather(pieces[2], 'fs', axis=0, tiled=True)  81.4 us
    all_gather x1, waiting for transfers between devices, local(): lax.all_gather(pieces[1], 'fs', axis=0, tiled=True)  80.8 us
    all_gather x1, blocking collectives, backward(): gain_total = lax.all_gather(gain_part, axis_name=('fs', 'tp')).sum(axis=0)  40.9 us
    dot_general x3, matrix products, transposed(): lax.dot_general(matrix_a, matrix_b, (((1,), (1,)), ((), ())), preferred_e...  32.1 us
    dot_general x2, matrix products, outer_sum(): lax.dot_general(matrix_a, matrix_b, (((0,), (0,)), ((), ())), preferred_e...  29.9 us
  transfers between devices with their start and end apart: 6, of which 4 were waited for; matrix products, arithmetic and copies ran while one was open for 19% of the time, Pallas kernels for 0%

profile of v1, /device:TPU:0, one launch (start us, length us, event | category | flops | bytes accessed | tf_op | source)
XLA Modules:
  0.0 707.5 jit_solution(12725325519416846717)
XLA Ops:
  7.2 0.0 all-gather.5.cloned.1.call-start
  7.2 0.7 all-gather.5.cloned.1.call-update
  7.9 0.0 all-gather.7.cloned.1.call-start
  7.9 0.7 all-gather.7.cloned.1.call-update
  8.7 0.0 all-gather.9.cloned.1.call-start
  8.7 0.7 all-gather.9.cloned.1.call-update
  9.4 0.0 reduce-scatter.4.cloned.1.call-start
  9.4 0.0 copy-start
  9.4 0.8 convert_element_type.59
  10.3 3.3 fusion.4
  13.6 0.0 copy-done
  13.6 0.9 fusion.13
  14.5 90.8 %all-gather.5.cloned.1.call-done = bf16[2048,1408]{1,0:T(8,128)(2,1)} async-done(((bf16[256,1408]{1,0:T(8,128)(2,1)}), bf16[2048,1408]{1,0:T(8,128)(2,1)}) %all-gather.5.cloned.1.call-update) | async-done | bytes 5767184 | tf_op jit(solution)/shard_map/all_gather | solution.py:110
  105.2 12.0 %fusion.20 = f32[1024,1408]{1,0:T(8,128)} fusion(bf16[2048,1408]{1,0:T(8,128)(2,1)} %all-gather.5.cloned.1.call-done, bf16[1024,2048]{1,0:T(8,128)(2,1)} %param.11, f32[2048]{0:T(1024)S(1)} %convert_element_type.59, f32[1024]{0:T(1024)S(1)} %add_rsqrt_fusion.1), kind=kOutput, calls=%fused_computation.38 | convolution fusion | flops 5913968640 | bytes 15740928 | tf_op jit(solution)/shard_map/dot_general | solution.py:36
  117.2 80.8 %all-gather.7.cloned.1.call-done = bf16[2048,1408]{1,0:T(8,128)(2,1)} async-done(((bf16[256,1408]{1,0:T(8,128)(2,1)}), bf16[2048,1408]{1,0:T(8,128)(2,1)}) %all-gather.7.cloned.1.call-update) | async-done | bytes 5767184 | tf_op jit(solution)/shard_map/all_gather | solution.py:111
  197.9 11.3 %multiply_convert_fusion.4 = bf16[1024,1408]{1,0:T(8,128)(2,1)S(1)} fusion(f32[1024,1408]{1,0:T(8,128)} %fusion.20, bf16[2048,1408]{1,0:T(8,128)(2,1)} %all-gather.7.cloned.1.call-done, bf16[1024,2048]{1,0:T(8,128)(2,1)} %param.11, f32[2048]{0:T(1024)S(1)} %convert_element_type.59, f32[1024]{0:T(1024)S(1)} %add_rsqrt_fusion.1), kind=kOutput, calls=%fused_computation.30 | convolution fusion | flops 5922619392 | bytes 18624512 | tf_op jit(solution)/shard_map/dot_general | solution.py:37
  209.2 0.0 copy-start.8
  209.3 81.4 %all-gather.9.cloned.1.call-done = bf16[2048,1408]{1,0:T(8,128)(2,1)} async-done(((bf16[256,1408]{1,0:T(8,128)(2,1)}), bf16[2048,1408]{1,0:T(8,128)(2,1)}) %all-gather.9.cloned.1.call-update) | async-done | bytes 5767184 | tf_op jit(solution)/shard_map/all_gather | solution.py:112
  290.6 10.9 %convolution_convert_fusion.1 = bf16[1024,2048]{1,0:T(8,128)(2,1)} fusion(bf16[1024,1408]{1,0:T(8,128)(2,1)S(1)} %multiply_convert_fusion.4, bf16[2048,1408]{1,0:T(8,128)(2,1)} %all-gather.9.cloned.1.call-done), kind=kOutput, calls=%fused_computation.32 | convolution fusion | flops 5907677184 | bytes 12845056 | tf_op jit(solution)/shard_map/dot_general | solution.py:18
  301.5 0.0 copy-done.8
  301.5 0.0 reduce-scatter.4.cloned.1.call-update
  301.5 0.2 reduce-scatter.6.cloned.1.call-start
  301.8 0.0 copy-start.1
  301.8 0.0 slice-start.2
  301.8 12.1 %fusion.26 = f32[1024,1408]{1,0:T(8,128)} fusion(bf16[2048,1408]{1,0:T(8,128)(2,1)} %all-gather.5.cloned.1.call-done, bf16[1024,2048]{1,0:T(8,128)(2,1)} %param.12, f32[1024]{0:T(1024)S(1)} %add_rsqrt_fusion, f32[2048]{0:T(1024)S(1)} %convert_element_type.59), kind=kOutput, calls=%fused_computation.44 | convolution fusion | flops 5913968640 | bytes 15740928 | tf_op jit(solution)/shard_map/dot_general | solution.py:52
  313.9 0.0 copy-done.1
  313.9 0.0 copy-start.6
  313.9 0.0 slice-start.3
  313.9 0.0 slice-start
  313.9 10.7 %fusion.28 = f32[1024,1408]{1,0:T(8,128)} fusion(bf16[2048,1408]{1,0:T(8,128)(2,1)} %all-gather.7.cloned.1.call-done, bf16[1024,2048]{1,0:T(8,128)(2,1)S(1)} %copy-done.1, f32[1024]{0:T(1024)S(1)} %add_rsqrt_fusion, f32[2048]{0:T(1024)S(1)} %convert_element_type.59), kind=kOutput, calls=%fused_computation.45 | convolution fusion | flops 5913968640 | bytes 15740928 | tf_op jit(solution)/shard_map/dot_general | solution.py:53
  324.6 0.0 slice-done.2
  324.6 0.0 copy-done.6
  324.6 0.0 slice-done.3
  324.7 0.0 slice-start.1
  324.7 12.3 %multiply_convert_fusion.2 = (bf16[1024,1408]{1,0:T(8,128)(2,1)S(1)}, bf16[1024,1408]{1,0:T(8,128)(2,1)}) fusion(f32[1024,1408]{1,0:T(8,128)} %fusion.26, f32[1024,1408]{1,0:T(8,128)} %fusion.28, bf16[1024,2048]{1,0:T(8,128)(2,1)S(1)} %copy-done.6, bf16[2048,1408]{1,0:T(8,128)(2,1)S(1)} %bitcast.18), kind=kOutput, calls=%fused_computation.26 | convolution fusion | flops 5925765120 | bytes 27262976 | tf_op jit(solution)/shard_map/dot_general | solution.py:58
  337.0 0.0 slice-done
  337.0 0.0 slice-done.1
  337.0 10.2 %fusion.30 = f32[1024,2048]{1,0:T(8,128)} fusion(bf16[1024,1408]{1,0:T(8,128)(2,1)} %get-tuple-element.10, bf16[2048,1408]{1,0:T(8,128)(2,1)S(1)} %bitcast.16), kind=kOutput, calls=%fused_computation.46 | convolution fusion | flops 5905580032 | bytes 17039360 | tf_op jit(solution)/shard_map/dot_general | solution.py:18
  347.2 11.1 %fusion.12 = (f32[2048]{0:T(1024)S(1)}, f32[1024]{0:T(1024)S(1)}, f32[1024,2048]{1,0:T(8,128)S(1)}) fusion(bf16[1024,2048]{1,0:T(8,128)(2,1)S(1)} %copy-done.1, f32[1024]{0:T(1024)S(1)} %add_rsqrt_fusion, f32[2048]{0:T(1024)S(1)} %convert_element_type.59, f32[1024,2048]{1,0:T(8,128)} %fusion.30, bf16[1024,1408]{1,0:T(8,128)(2,1)S(1)} %get-tuple-element.9, ...), kind=kOutput, calls=%fused_computation.19 | convolution fusion | flops 5922354176 | bytes 29646848 | tf_op jit(solution)/shard_map/dot_general | solution.py:18
  358.3 3.5 fusion.11
  361.8 0.0 reduce-scatter.6.cloned.1.call-update
  361.8 0.0 reduce-scatter.8.cloned.1.call-start
  361.8 0.0 copy-start.2
  361.8 13.0 %fusion.14 = bf16[2048,1408]{1,0:T(8,128)(2,1)S(1)} fusion(bf16[1024,2048]{1,0:T(8,128)(2,1)} %param.13, f32[1024,1408]{1,0:T(8,128)} %fusion.28, f32[1024,1408]{1,0:T(8,128)} %fusion.26), kind=kOutput, calls=%fused_computation.21 | convolution fusion | flops 5919997952 | bytes 21495808 | tf_op jit(solution)/shard_map/dot_general | solution.py:24
  374.8 0.0 copy-done.2
  374.8 17.0 %convolution_convert_fusion = bf16[2048,2816]{1,0:T(8,128)(2,1)} fusion(bf16[1024,1408]{1,0:T(8,128)(2,1)S(1)} %get-tuple-element.9, bf16[1024,1408]{1,0:T(8,128)(2,1)} %get-tuple-element.10, bf16[1024,2048]{1,0:T(8,128)(2,1)S(1)} %copy-done.2, f32[1024]{0:T(1024)S(1)} %add_rsqrt_fusion, f32[2048]{0:T(1024)S(1)} %convert_element_type.59), kind=kOutput, calls=%fused_computation.2 | convolution fusion | flops 11836850176 | bytes 21508096 | tf_op jit(solution)/shard_map/dot_general | solution.py:24
  391.8 11.7 %pad_maximum_fusion = bf16[2048,4224]{1,0:T(8,128)(2,1)} fusion(bf16[2048,1408]{1,0:T(8,128)(2,1)S(1)} %fusion.14, bf16[2048,2816]{1,0:T(8,128)(2,1)} %convolution_convert_fusion), kind=kLoop, calls=%fused_computation | loop fusion | flops 34603008 | bytes 34603008 | tf_op jit(solution)/shard_map/concatenate | solution.py:78
  403.6 0.0 copy-start.7
  403.6 0.0 reduce-scatter.8.cloned.1.call-update
  403.6 40.9 %all-gather = f32[65536]{0:T(1024)S(1)} all-gather(f32[2048]{0:T(1024)S(1)} %get-tuple-element.7), channel_id=2, replica_groups=mesh['fs'=8,'tp'=4] {'fs','tp'}, dimensions={0}, use_global_device_ids=true | all-gather | bytes 270336 | tf_op jit(solution)/shard_map/all_gather | solution.py:88
  444.5 0.0 copy-done.7
  444.5 0.6 add.69
  445.1 0.0 copy-start.3
  445.1 0.0 copy-start.4
  445.2 0.0 reduce-scatter.4.cloned.1.call-done
  445.2 3.1 add_convert_fusion.1
  448.2 0.0 reduce-scatter.6.cloned.1.call-done
  448.2 2.9 add_convert_fusion
  451.1 245.3 %reduce-scatter.8.cloned.1.call-done = bf16[256,4224]{1,0:T(8,128)(2,1)} async-done(((bf16[2048,4224]{1,0:T(8,128)(2,1)}), bf16[256,4224]{1,0:T(8,128)(2,1)}) %reduce-scatter.8.cloned.1.call-update) | async-done | bytes 2162704 | tf_op jit(solution)/shard_map/reduce_scatter | solution.py:77
  696.4 2.0 convert_element_type.74
  698.4 0.0 copy-done.3
  698.4 0.0 copy-done.4
  698.4 0.0 copy-done.5
  698.4 2.3 slice_add_fusion
  (8 shorter events, 0.1 us)
Async XLA Ops:
  7.2 98.1 %all-gather.5.cloned.1.call-start = ((), (), s32[]{:S(2)}) async-start(), calls=%async_computation.3 | async-start | bytes 6488064 | tf_op jit(solution)/shard_map/all_gather | solution.py:110
  7.9 190.0 %all-gather.7.cloned.1.call-start = ((), (), s32[]{:S(2)}) async-start(), calls=%async_computation.4 | async-start | bytes 6488064 | tf_op jit(solution)/shard_map/all_gather | solution.py:111
  8.7 282.0 %all-gather.9.cloned.1.call-start = ((), (), s32[]{:S(2)}) async-start(), calls=%async_computation.5 | async-start | bytes 6488064 | tf_op jit(solution)/shard_map/all_gather | solution.py:112
  9.4 435.8 %reduce-scatter.4.cloned.1.call-start = ((), (), s32[]{:S(2)}) async-start(), calls=%async_computation.6 | async-start | bytes 5242880 | tf_op jit(solution)/shard_map/reduce_scatter | solution.py:40
  9.4 4.1 copy-start
  209.2 92.3 %copy-start.8 = (bf16[1024,1408]{1,0:T(8,128)(2,1)}, bf16[1024,1408]{1,0:T(8,128)(2,1)S(1)}, u32[]{:S(2)}) copy-start(bf16[1024,1408]{1,0:T(8,128)(2,1)S(1)} %multiply_convert_fusion.4) | copy-start | bytes 8650756
  301.5 146.7 %reduce-scatter.6.cloned.1.call-start = ((), (), s32[]{:S(2)}) async-start(), calls=%async_computation.7 | async-start | bytes 5242880 | tf_op jit(solution)/shard_map/reduce_scatter | solution.py:71
  301.8 12.2 %copy-start.1 = (bf16[1024,2048]{1,0:T(8,128)(2,1)S(1)}, bf16[1024,2048]{1,0:T(8,128)(2,1)}, u32[]{:S(2)}) copy-start(bf16[1024,2048]{1,0:T(8,128)(2,1)} %param.12) | copy-start | bytes 12582916
  301.8 22.9 %slice-start.2 = ((s8[5767168]{0:T(1024)(128)(4,1)}), s8[4194304]{0:T(1024)(128)(4,1)S(1)}, s32[]{:S(2)}) async-start(s8[5767168]{0:T(1024)(128)(4,1)} %bitcast.17), calls=%async_computation.11 | async-start | bytes 8388608
  313.9 10.7 %copy-start.6 = (bf16[1024,2048]{1,0:T(8,128)(2,1)S(1)}, bf16[1024,2048]{1,0:T(8,128)(2,1)}, u32[]{:S(2)}) copy-start(bf16[1024,2048]{1,0:T(8,128)(2,1)} %param.13) | copy-start | bytes 12582916
  313.9 10.7 %slice-start.3 = ((s8[5767168]{0:T(1024)(128)(4,1)}), s8[1572864]{0:T(1024)(128)(4,1)S(1)}, s32[]{:S(2)}) async-start(s8[5767168]{0:T(1024)(128)(4,1)} %bitcast.17), calls=%async_computation.12 | async-start | bytes 3145728
  313.9 23.0 %slice-start = ((s8[5767168]{0:T(1024)(128)(4,1)}), s8[4194304]{0:T(1024)(128)(4,1)S(1)}, s32[]{:S(2)}) async-start(s8[5767168]{0:T(1024)(128)(4,1)} %bitcast.15), calls=%async_computation.9 | async-start | bytes 8388608
  324.7 12.3 %slice-start.1 = ((s8[5767168]{0:T(1024)(128)(4,1)}), s8[1572864]{0:T(1024)(128)(4,1)S(1)}, s32[]{:S(2)}) async-start(s8[5767168]{0:T(1024)(128)(4,1)} %bitcast.15), calls=%async_computation.10 | async-start | bytes 3145728
  361.8 334.6 %reduce-scatter.8.cloned.1.call-start = ((), (), s32[]{:S(2)}) async-start(), calls=%async_computation.8 | async-start | bytes 19464192 | tf_op jit(solution)/shard_map/reduce_scatter | solution.py:77
  361.8 13.0 %copy-start.2 = (bf16[1024,2048]{1,0:T(8,128)(2,1)S(1)}, bf16[1024,2048]{1,0:T(8,128)(2,1)}, u32[]{:S(2)}) copy-start(bf16[1024,2048]{1,0:T(8,128)(2,1)} %param.12) | copy-start | bytes 12582916
  403.6 41.0 %copy-start.7 = (f32[2048]{0:T(1024)S(1)}, f32[2048]{0:T(1024)}, u32[]{:S(2)}) copy-start(f32[2048]{0:T(1024)} %param.21) | copy-start | bytes 24580
  445.1 253.3 %copy-start.3 = (f32[256,1408]{1,0:T(8,128)S(1)}, f32[256,1408]{1,0:T(8,128)}, u32[]{:S(2)}) copy-start(f32[256,1408]{1,0:T(8,128)} %param.20) | copy-start | bytes 4325380
  445.1 253.3 %copy-start.4 = (f32[256,1408]{1,0:T(8,128)S(1)}, f32[256,1408]{1,0:T(8,128)}, u32[]{:S(2)}) copy-start(f32[256,1408]{1,0:T(8,128)} %param.19) | copy-start | bytes 4325380
  696.4 2.0 copy-start.5
Sparse Core Ops, SparseCore 0:
  10.2 95.0 all-gather.4
  107.4 90.4 all-gather.6
  200.1 90.4 all-gather.8
  301.6 42.7 reduce-scatter.3
  361.9 42.7 reduce-scatter.5
  408.5 287.8 reduce-scatter.7
